TPU v7x, 256 devices: a whole 4x4x8 slice. The times are simulated.
256 devices in a mesh: sp: 32 (over z, x), tp: 8 (over y, core).
Axes of the slice: x: 4, y: 4, z: 8, core: 2. Of those that a mesh axis runs over, the one named last changes fastest.
Arguments:
- tokens: bfloat16 [32768, 2048], P('sp', 'tp'), may hold values from -70 to 70
- w_query: bfloat16 [2048, 1024], P(None, 'tp'), may hold values from -0.125 to 0.125
- w_key: bfloat16 [2048, 1024], P(None, 'tp'), may hold values from -0.125 to 0.125
- w_value: bfloat16 [2048, 1024], P(None, 'tp'), may hold values from -0.125 to 0.125
- w_delta_gate: bfloat16 [2048, 1024], P(None, 'tp'), may hold values from -0.125 to 0.125
- w_glu_value: bfloat16 [2048, 1024], P(None, 'tp'), may hold values from -0.125 to 0.125
- w_glu_gate: bfloat16 [2048, 1024], P(None, 'tp'), may hold values from -0.125 to 0.125
- w_conv_gate: bfloat16 [2048, 1024], P(None, 'tp'), may hold values from -0.125 to 0.125
- w_beta: bfloat16 [2048, 8], replicated, may hold values from -0.125 to 0.125
- w_decay: bfloat16 [2048, 8], replicated, may hold values from -0.125 to 0.125
- decay_log: float32 [8], replicated, may hold values from -12 to -3
- head_gain: float32 [128], replicated, may hold values from 0.1 to 1.9
- conv_taps: bfloat16 [31, 1024], P(None, 'tp'), may hold values from -2.5 to 2.5
- ln_gain: float32 [1024], P('tp'), may hold values from 0.1 to 1.9
- ln_shift: float32 [1024], P('tp'), may hold values from -3 to 3
- out_delta: bfloat16 [1024, 2048], P('tp'), may hold values from -0.125 to 0.125
- out_conv: bfloat16 [1024, 2048], P('tp'), may hold values from -0.125 to 0.125
Outputs:
- mixed_out: bfloat16 [32768, 2048], P(('sp', 'tp'))
All inputs are finite; a program needn't handle non-finite values.
Results may differ from a plain program's by a relative error of at most 0.024.
Values may be sent and summed in bfloat16 or wider, within the bound.
No kernel may reach another device: no remote copies, remote signals or barrier semaphores. Data moves between devices by JAX's collectives and lax.ppermute only.
A program may use at most 64 MiB of HBM per device.

v0:
```python
import jax
import jax.numpy as jnp
from jax import lax
from jax.sharding import Mesh
from jax.sharding import PartitionSpec as P

SPAN = 64
SP = ("sp_0", "sp_1")
SP_TP = ("sp_0", "sp_1", "tp")
TINY_NORM = 1e-06
TINY_VAR = 1e-05


def filled_with(shard, identity):
    return jnp.broadcast_to(jnp.asarray(identity, shard.dtype), shard.shape)


def prefix_by_axis(shard, axes, combine, identity):
    before = start = filled_with(shard, identity)
    so_far = shard
    for axis in reversed(axes):
        count, mine = (lax.axis_size(axis), lax.axis_index(axis))
        pieces = lax.all_gather(so_far, axis)
        inside, so_far = (start, start)
        for k in range(count):
            passed = k < mine
            so_far = combine(so_far, pieces[k])
            inside = jnp.where(passed, so_far, inside)
        before = combine(inside, before)
    return before


def shifted(block, axis, distance):
    devices = range(lax.axis_size(axis))
    route = [(i - distance, i) for i in devices if i - distance in devices]
    return lax.ppermute(block, axis, route)


def sent_to_all(shard, axis):
    count = lax.axis_size(axis)
    return lax.all_to_all(
        jnp.broadcast_to(shard[None], (count, *shard.shape)), axis, 0, 0, tiled=True
    )


def over_copies(shard, axis):
    return sent_to_all(shard, axis).sum(axis=0)


def packed_total(arrays, axis):
    ends = [0]
    for a in arrays:
        ends.append(ends[-1] + a.size)
    so_far = over_copies(jnp.concatenate([a.ravel() for a in arrays]), axis)
    return tuple((so_far[b:e].reshape(a.shape) for a, b, e in zip(arrays, ends, ends[1:])))


def block_terms(query, keys, values, strength, log_decay):
    log_sum = jnp.cumsum(log_decay, axis=-1)
    offsets = jnp.arange(SPAN)
    causal = offsets[:, None] >= offsets[None, :]
    strict = offsets[:, None] > offsets[None, :]
    spread = log_sum[..., :, None] - log_sum[..., None, :]
    damping = jnp.where(causal, jnp.exp(jnp.where(causal, spread, 0.0)), 0.0)
    scaled_keys = keys * strength[..., None]
    lower = jnp.where(strict, jnp.einsum("hnid,hnjd->hnij", scaled_keys, keys) * damping, 0.0)
    identity = jnp.eye(SPAN, dtype=jnp.float32)
    right = jnp.concatenate(
        [values * strength[..., None], scaled_keys * jnp.exp(log_sum)[..., None]], axis=-1
    )
    solved = jax.scipy.linalg.solve_triangular(
        identity + lower, right, lower=True, unit_diagonal=True
    )
    width = values.shape[-1]
    scores = jnp.einsum("hnid,hnjd->hnij", query, keys) * damping
    return (log_sum, solved[..., :width], solved[..., width:], scores)


def local(
    tokens,
    w_query,
    w_key,
    w_value,
    w_delta_gate,
    w_glu_value,
    w_glu_gate,
    w_conv_gate,
    w_beta,
    w_decay,
    decay_log,
    head_gain,
    conv_taps,
    ln_gain,
    ln_shift,
    out_delta,
    out_conv,
):
    rows_here = tokens.shape[0]
    tp_size = lax.axis_size("tp")
    width_all = tokens.shape[1] * tp_size
    weights = (
        w_query,
        w_key,
        w_value,
        w_delta_gate,
        w_glu_value,
        w_glu_gate,
        w_conv_gate,
        w_beta,
        w_decay,
    )
    piece = lax.all_gather(tokens, "tp", axis=1, tiled=True)
    totals = tuple(
        (jnp.dot(piece, weight, preferred_element_type=jnp.float32) for weight in weights)
    )
    squares = jnp.sum(jnp.square(piece.astype(jnp.float32)), axis=1)
    sums, squares = (totals, squares)
    inv_rms = lax.rsqrt(squares / width_all + TINY_NORM)[:, None]
    scaled = [summed * inv_rms for summed in sums]
    query_raw, key_raw, value_raw, delta_gate_raw, glu_value_raw, glu_gate_raw, conv_gate_raw = [
        item.astype(jnp.bfloat16) for item in scaled[:7]
    ]
    head_size = head_gain.shape[0]
    heads_here = w_query.shape[1] // head_size
    first_head = lax.axis_index("tp") * heads_here
    strength = jax.nn.sigmoid(lax.dynamic_slice_in_dim(scaled[7], first_head, heads_here, 1))
    rates = jnp.exp(lax.dynamic_slice_in_dim(decay_log, first_head, heads_here, 0))
    log_decay = -rates[None, :] * jax.nn.softplus(
        lax.dynamic_slice_in_dim(scaled[8], first_head, heads_here, 1)
    )
    blocks = rows_here // SPAN

    def to_blocks(raw):
        return jnp.transpose(raw.reshape(blocks, SPAN, heads_here, head_size), (2, 0, 1, 3))

    def unit_rows(array):
        return array * lax.rsqrt(jnp.sum(array * array, axis=-1, keepdims=True) + TINY_NORM)

    query = unit_rows(to_blocks(query_raw.astype(jnp.float32))) * head_size ** (-0.5)
    keys = unit_rows(to_blocks(key_raw.astype(jnp.float32)))
    values = to_blocks(value_raw.astype(jnp.float32))
    strength_blocks = jnp.transpose(strength.reshape(blocks, SPAN, heads_here), (2, 0, 1))
    decay_blocks = jnp.transpose(log_decay.reshape(blocks, SPAN, heads_here), (2, 0, 1))
    log_sum, corrected, key_terms, scores = block_terms(
        query, keys, values, strength_blocks, decay_blocks
    )

    def advance(memory, inputs):
        query_block, keys_block, corrected_block, terms_block, scores_block, log_block = inputs
        extended = jnp.concatenate([jnp.zeros_like(corrected_block), corrected_block], axis=-1)
        fresh = extended - jnp.einsum("hcd,hde->hce", terms_block, memory)
        output = jnp.einsum("hcd,hde->hce", query_block * jnp.exp(log_block)[..., None], memory)
        output = output + jnp.einsum("hcs,hse->hce", scores_block, fresh)
        tail_log = log_block[:, -1:]
        weighted = keys_block * jnp.exp(tail_log - log_block)[..., None]
        memory = memory * jnp.exp(tail_log)[..., None] + jnp.einsum("hcd,hce->hde", weighted, fresh)
        return (memory, output)

    start_state = jnp.concatenate(
        [
            jnp.broadcast_to(
                jnp.eye(head_size, dtype=jnp.float32), (heads_here, head_size, head_size)
            ),
            jnp.zeros((heads_here, head_size, head_size), jnp.float32),
        ],
        axis=-1,
    )
    sequence_inputs = tuple(
        (jnp.moveaxis(item, 1, 0) for item in (query, keys, corrected, key_terms, scores, log_sum))
    )
    final, outputs = lax.scan(advance, start_state, sequence_inputs)
    outputs = jnp.moveaxis(outputs, 0, 1).reshape(heads_here, rows_here, 2 * head_size)

    def compose(earlier, later):
        moved = jnp.einsum("hij,hjk->hik", later[..., :head_size], earlier)
        return moved + jnp.concatenate(
            [jnp.zeros_like(later[..., :head_size]), later[..., head_size:]], axis=-1
        )

    prefix = prefix_by_axis(final, SP, compose, start_state)
    carried = prefix[..., head_size:]
    result = outputs[..., head_size:] + jnp.einsum(
        "htd,hde->hte", outputs[..., :head_size], carried
    )
    result = jnp.transpose(result, (1, 0, 2))
    result = (
        result
        * lax.rsqrt(jnp.mean(result * result, axis=-1, keepdims=True) + TINY_NORM)
        * head_gain
    )
    delta_mixed = (
        result.reshape(rows_here, heads_here * head_size)
        * jax.nn.silu(delta_gate_raw.astype(jnp.float32))
    ).astype(jnp.bfloat16)
    kernel = conv_taps.shape[0]
    channels = conv_taps.shape[1]
    gated_units = (
        glu_value_raw.astype(jnp.float32) * jax.nn.sigmoid(glu_gate_raw.astype(jnp.float32))
    ).astype(jnp.bfloat16)
    before = shifted(gated_units[rows_here - (kernel - 1) :], SP, 1)
    padded = jnp.concatenate([before, gated_units], axis=0)
    filtered = jnp.zeros((rows_here, channels), jnp.float32)
    for offset in range(kernel):
        filtered = filtered + padded[offset : offset + rows_here].astype(jnp.float32) * conv_taps[
            offset
        ].astype(jnp.float32)
    first_sum = jnp.sum(filtered, axis=1)
    second_sum = jnp.sum(filtered * filtered, axis=1)
    first_sum, second_sum = packed_total((first_sum, second_sum), "tp")
    channels_all = channels * tp_size
    center = first_sum / channels_all
    variance = jnp.maximum(second_sum / channels_all - center * center, 0.0)
    normed = (filtered - center[:, None]) * lax.rsqrt(variance + TINY_VAR)[
        :, None
    ] * ln_gain + ln_shift
    conv_mixed = (jax.nn.silu(normed) * jax.nn.silu(conv_gate_raw.astype(jnp.float32))).astype(
        jnp.bfloat16
    )
    summed = jnp.dot(delta_mixed, out_delta, preferred_element_type=jnp.float32)
    return lax.psum_scatter(
        (summed + jnp.dot(conv_mixed, out_conv, preferred_element_type=jnp.float32)).astype(
            jnp.bfloat16
        ),
        "tp",
        scatter_dimension=0,
        tiled=True,
    )


def solution(mesh):
    finer = Mesh(mesh.devices.reshape(8, 4, mesh.shape["tp"]), ("sp_0", "sp_1", "tp"))
    placed = (
        P(SP, "tp"),
        P(None, "tp"),
        P(None, "tp"),
        P(None, "tp"),
        P(None, "tp"),
        P(None, "tp"),
        P(None, "tp"),
        P(None, "tp"),
        P(),
        P(),
        P(),
        P(),
        P(None, "tp"),
        P("tp"),
        P("tp"),
        P("tp", None),
        P("tp", None),
    )
    return jax.shard_map(
        local, mesh=finer, in_specs=placed, out_specs=P(SP_TP, None), check_vma=False
    )
```

profile of v0, /device:TPU:2, one launch (start us, length us, event | category | flops | bytes accessed | tf_op | source)
XLA Modules:
  0.0 365.5 jit_solution(16131292923218178079)
XLA Ops:
  9.4 1.7 bitcast_convert_fusion.30
  11.1 39.1 %all-gather.5.cloned.1.call-done = bf16[1024,2048]{1,0:T(8,128)(2,1)} async-done(((bf16[1024,256]{1,0:T(8,128)(2,1)}), bf16[1024,2048]{1,0:T(8,128)(2,1)}) %all-gather.5.cloned.1.call-update) | async-done | bytes 4194320 | tf_op jit(solution)/shard_map/all_gather | solution.py:112
  50.2 3.2 multiply_reduce_fusion
  56.5 3.5 multiply_reduce_fusion.4
  60.8 78.6 %custom-call.4 = f32[16,1,64,64]{2,3,1,0:T(8,128)S(1)} custom-call(f32[16,1,64,64]{3,2,1,0:T(8,128)S(1)} %fusion.30), custom_call_target="InvertDiagBlocksLowerTriangular" | custom-call | tf_op jit(solution)/shard_map/jit(_solve_triangular)/vmap()/triangular_solve | solution.py:71
  139.5 3.6 fusion.34
  149.1 84.6 %while.12 = (s32[]{:T(128)}, f32[1,128,256]{2,1,0:T(8,128)S(1)}, f32[16,1,64,256]{3,2,1,0:T(8,128)}, f32[16,1,64]{2,1,0:T(1,128)}, f32[16,1,64,128]{3,2,1,0:T(8,...) while((s32[]{:T(128)}, f32[1,128,256]{2,1,0:T(8,128)S(1)}, ...), condition=%wide.region_5.6_spmd, body=%wide.region_4.5_spmd.sunk | while | flops 14811202 | bytes 1019293 | solution.py:171
  152.9 1.5 fusion.250
  158.2 1.5 fusion.250
  163.5 1.5 fusion.250
  168.7 1.5 fusion.250
  174.1 1.5 fusion.250
  179.3 1.5 fusion.250
  189.9 1.5 fusion.250
  195.2 1.5 fusion.250
  205.6 1.5 fusion.250
  211.0 1.5 fusion.250
  216.1 1.5 fusion.250
  221.5 1.5 fusion.250
  226.9 1.5 fusion.250
  233.7 13.6 %all-gather = f32[4,128,256]{2,1,0:T(8,128)S(1)} all-gather(f32[1,128,256]{2,1,0:T(8,128)S(1)} %get-tuple-element.54), channel_id=2, replica_groups=mesh['sp_0'=8,'sp_1'=4,'tp'=8] {'sp_1'}, dimensions={0}, use_global_device_ids=true | all-gather | bytes 655360 | tf_op jit(solution)/shard_map/all_gather | solution.py:23
  248.6 3.6 fusion.48
  253.7 2.1 collective-permute-start
  255.9 3.6 collective-permute-done
  259.6 2.7 fusion.188
  263.0 3.9 %all-to-all-start = ((f32[8,1,2048]{2,1,0:T(1,128)}), f32[8,1,2048]{2,1,0:T(1,128)S(1)}, u32[]{:S(2)}, u32[]{:S(2)}) async-start(f32[8,1,2048]{2,1,0:T(1,128)} %broadcast_in_dim.36), calls=%async_computation | async-start | bytes 131072 | tf_op jit(solution)/shard_map/all_to_all | solution.py:41
  267.2 5.4 %all-to-all-done = f32[8,1,2048]{2,1,0:T(1,128)S(1)} async-done(((f32[8,1,2048]{2,1,0:T(1,128)}), f32[8,1,2048]{2,1,0:T(1,128)S(1)}, u32[]{:S(2)}, u32[]{:S(2)}) %all-to-all-start) | async-done | bytes 65568 | tf_op jit(solution)/shard_map/all_to_all | solution.py:41
  272.6 15.2 %all-gather.7.cloned.1.call-done = f32[8,128,256]{2,1,0:T(8,128)} async-done(((f32[1,128,256]{2,1,0:T(8,128)}), f32[8,128,256]{2,1,0:T(8,128)}) %all-gather.7.cloned.1.call-update) | async-done | bytes 1048592 | tf_op jit(solution)/shard_map/all_gather | solution.py:23
  295.8 1.8 convolution_bitcast_fusion.4
  298.9 9.9 %fusion.81 = f32[1024,2048]{1,0:T(8,128)} fusion(bf16[128,2048]{1,0:T(8,128)(2,1)S(1)} %copy-done, f32[1,1024,128]{2,1,0:T(8,128)S(1)} %get-tuple-element.168, bf16[1024,2048]{1,0:T(8,128)(2,1)} %all-gather.5.cloned.1.call-done, bf16[2048,128]{1,0:T(8,128)(2,1)S(1)} %copy-done.8, f32[128]{0:T(128)S(1)} %copy-done.44, f32[1024]{0:T(1024)S(1)} %add_rsqrt_fusion, ...), kind=kOutput, calls=%fused_computation.153 | convolution fusion | flops 1075183616 | bytes 14164480 | tf_op jit(solution)/shard_map/dot_general | solution.py:219
  308.9 11.0 %add_convert_fusion = bf16[1024,2048]{1,0:T(8,128)(2,1)} fusion(f32[1024,2048]{1,0:T(8,128)} %fusion.81, bf16[128,2048]{1,0:T(8,128)(2,1)S(1)} %copy-done.6, bf16[1024,2048]{1,0:T(8,128)(2,1)} %all-gather.5.cloned.1.call-done, bf16[2048,128]{1,0:T(8,128)(2,1)S(1)} %copy-done.7, f32[1024,128]{1,0:T(8,128)S(1)} %get-tuple-element.113, f32[128]{0:T(128)S(1)} %copy-done.42, ...), kind=kOutput, calls=%fused_computation.32 | convolution fusion | flops 1080164352 | bytes 18363392 | tf_op jit(solution)/shard_map/dot_general | solution.py:221
  319.9 39.1 %reduce-scatter.2.cloned.1.call-done = bf16[128,2048]{1,0:T(8,128)(2,1)} async-done(((bf16[1024,2048]{1,0:T(8,128)(2,1)}), bf16[128,2048]{1,0:T(8,128)(2,1)}) %reduce-scatter.2.cloned.1.call-update) | async-done | bytes 524304 | tf_op jit(solution)/shard_map/reduce_scatter | solution.py:220
  (269 shorter events, 79.6 us)
Async XLA Ops:
  6.5 292.3 %copy-start = (bf16[128,2048]{1,0:T(8,128)(2,1)S(1)}, bf16[128,2048]{1,0:T(8,128)(2,1)}, u32[]{:S(2)}) copy-start(bf16[128,2048]{1,0:T(8,128)(2,1)} %param.34) | copy-start | bytes 1572868
  6.5 46.9 %copy-start.18 = (bf16[2048,8]{0,1:T(8,128)(2,1)S(1)}, bf16[2048,8]{0,1:T(8,128)(2,1)}, u32[]{:S(2)}) copy-start(bf16[2048,8]{0,1:T(8,128)(2,1)} %param.27) | copy-start | bytes 98308
  6.5 43.7 %all-gather.5.cloned.1.call-start = ((), (), s32[]{:S(2)}) async-start(), calls=%async_computation.2 | async-start | bytes 4718592 | tf_op jit(solution)/shard_map/all_gather | solution.py:112
  7.3 280.5 %all-gather.7.cloned.1.call-start = ((), (), s32[]{:S(2)}) async-start(), calls=%async_computation.4 | async-start | bytes 1179648 | tf_op jit(solution)/shard_map/all_gather | solution.py:23
  9.3 50.8 %copy-start.21 = (pred[64,64]{1,0:T(8,128)(4,1)}, pred[64,64]{1,0:T(8,128)(4,1)S(1)}, u32[]{:S(2)}) copy-start(pred[64,64]{1,0:T(8,128)(4,1)S(1)} %get-tuple-element.169) | copy-start | bytes 12292
  53.7 85.8 %copy-start.10 = (f32[1024]{0:T(1024)}, f32[1024]{0:T(1024)S(1)}, u32[]{:S(2)}) copy-start(f32[1024]{0:T(1024)S(1)} %add_rsqrt_fusion.3) | copy-start | bytes 12292
  60.1 83.0 %copy-start.13 = (f32[16,64]{1,0:T(8,128)}, f32[16,64]{1,0:T(8,128)S(1)}, u32[]{:S(2)}) copy-start(f32[16,64]{1,0:T(8,128)S(1)} %rsqrt.42) | copy-start | bytes 12292
  149.0 99.5 %copy-start.12 = (f32[1024]{0:T(1024)S(1)}, f32[1024]{0:T(1024)}, u32[]{:S(2)}) copy-start(f32[1024]{0:T(1024)} %copy-done.10) | copy-start | bytes 12292
  149.0 99.5 %copy-start.47 = (bf16[2048,128]{1,0:T(8,128)(2,1)S(1)}, bf16[2048,128]{1,0:T(8,128)(2,1)}, u32[]{:S(2)}) copy-start(bf16[2048,128]{1,0:T(8,128)(2,1)} %param.25) | copy-start | bytes 1572868
  252.2 7.2 %copy-start.23 = (f32[128]{0:T(128)S(1)}, f32[128]{0:T(128)}, u32[]{:S(2)}) copy-start(f32[128]{0:T(128)} %get-tuple-element.130) | copy-start | bytes 1540
  252.2 7.2 %copy-start.24 = (f32[128]{0:T(128)S(1)}, f32[128]{0:T(128)}, u32[]{:S(2)}) copy-start(f32[128]{0:T(128)} %get-tuple-element.131) | copy-start | bytes 1540
  252.3 7.2 %copy-start.25 = (f32[128]{0:T(128)S(1)}, f32[128]{0:T(128)}, u32[]{:S(2)}) copy-start(f32[128]{0:T(128)} %get-tuple-element.132) | copy-start | bytes 1540
  252.3 7.2 %copy-start.26 = (f32[128]{0:T(128)S(1)}, f32[128]{0:T(128)}, u32[]{:S(2)}) copy-start(f32[128]{0:T(128)} %get-tuple-element.133) | copy-start | bytes 1540
  252.3 7.2 %copy-start.27 = (f32[128]{0:T(128)S(1)}, f32[128]{0:T(128)}, u32[]{:S(2)}) copy-start(f32[128]{0:T(128)} %get-tuple-element.134) | copy-start | bytes 1540
  252.3 7.2 %copy-start.28 = (f32[128]{0:T(128)S(1)}, f32[128]{0:T(128)}, u32[]{:S(2)}) copy-start(f32[128]{0:T(128)} %get-tuple-element.135) | copy-start | bytes 1540
  252.3 7.2 %copy-start.29 = (f32[128]{0:T(128)S(1)}, f32[128]{0:T(128)}, u32[]{:S(2)}) copy-start(f32[128]{0:T(128)} %get-tuple-element.136) | copy-start | bytes 1540
  252.3 7.2 %copy-start.30 = (f32[128]{0:T(128)S(1)}, f32[128]{0:T(128)}, u32[]{:S(2)}) copy-start(f32[128]{0:T(128)} %get-tuple-element.137) | copy-start | bytes 1540
  252.3 7.2 %copy-start.31 = (f32[128]{0:T(128)S(1)}, f32[128]{0:T(128)}, u32[]{:S(2)}) copy-start(f32[128]{0:T(128)} %get-tuple-element.138) | copy-start | bytes 1540
  252.3 7.2 %copy-start.32 = (f32[128]{0:T(128)S(1)}, f32[128]{0:T(128)}, u32[]{:S(2)}) copy-start(f32[128]{0:T(128)} %get-tuple-element.139) | copy-start | bytes 1540
  252.3 7.2 %copy-start.33 = (f32[128]{0:T(128)S(1)}, f32[128]{0:T(128)}, u32[]{:S(2)}) copy-start(f32[128]{0:T(128)} %get-tuple-element.140) | copy-start | bytes 1540
  252.3 7.2 %copy-start.34 = (f32[128]{0:T(128)S(1)}, f32[128]{0:T(128)}, u32[]{:S(2)}) copy-start(f32[128]{0:T(128)} %get-tuple-element.141) | copy-start | bytes 1540
  252.4 14.5 %copy-start.4 = (f32[1,128,256]{2,1,0:T(8,128)S(1)}, f32[1,128,256]{2,1,0:T(8,128)}, u32[]{:S(2)}) copy-start(f32[1,128,256]{2,1,0:T(8,128)} %fusion.53) | copy-start | bytes 393220
  253.7 43.9 %copy-start.9 = (f32[16,1,64,256]{3,2,1,0:T(8,128)S(1)}, f32[16,1,64,256]{3,2,1,0:T(8,128)}, u32[]{:S(2)}) copy-start(f32[16,1,64,256]{3,2,1,0:T(8,128)} %get-tuple-element.53) | copy-start | bytes 3145732
  253.7 45.2 %copy-start.8 = (bf16[2048,128]{1,0:T(8,128)(2,1)S(1)}, bf16[2048,128]{1,0:T(8,128)(2,1)}, u32[]{:S(2)}) copy-start(bf16[2048,128]{1,0:T(8,128)(2,1)} %param.23) | copy-start | bytes 1572868
  253.7 45.2 %copy-start.44 = (f32[128]{0:T(128)S(1)}, f32[128]{0:T(128)}, u32[]{:S(2)}) copy-start(f32[128]{0:T(128)} %param.30) | copy-start | bytes 1540
  253.7 5.7 %collective-permute-start = (bf16[30,128]{1,0:T(8,128)(2,1)S(1)}, bf16[30,128]{1,0:T(8,128)(2,1)S(1)}, u32[]{:S(2)}, u32[]{:S(2)}) collective-permute-start(bf16[30,128]{1,0:T(8,128)(2,1)S(1)} %slice.504), channel_id=1, source_target_pairs={{0,8},{8,16},{16,24},{24,32},{32,40},{40,48},{48,56},{56,64},{64,7... | collective-permute-start | bytes 23048 | tf_op jit(solution)/shard_map/ppermute | solution.py:36
  263.0 9.6 %all-to-all-start = ((f32[8,1,2048]{2,1,0:T(1,128)}), f32[8,1,2048]{2,1,0:T(1,128)S(1)}, u32[]{:S(2)}, u32[]{:S(2)}) async-start(f32[8,1,2048]{2,1,0:T(1,128)} %broadcast_in_dim.36), calls=%async_computation | async-start | bytes 131072 | tf_op jit(solution)/shard_map/all_to_all | solution.py:41
  266.9 92.1 %reduce-scatter.2.cloned.1.call-start = ((), (), s32[]{:S(2)}) async-start(), calls=%async_computation.3 | async-start | bytes 4718592 | tf_op jit(solution)/shard_map/reduce_scatter | solution.py:220
  298.9 10.0 %copy-start.6 = (bf16[128,2048]{1,0:T(8,128)(2,1)S(1)}, bf16[128,2048]{1,0:T(8,128)(2,1)}, u32[]{:S(2)}) copy-start(bf16[128,2048]{1,0:T(8,128)(2,1)} %param.35) | copy-start | bytes 1572868
  298.9 10.0 %copy-start.7 = (bf16[2048,128]{1,0:T(8,128)(2,1)S(1)}, bf16[2048,128]{1,0:T(8,128)(2,1)}, u32[]{:S(2)}) copy-start(bf16[2048,128]{1,0:T(8,128)(2,1)} %param.26) | copy-start | bytes 1572868
  298.9 9.9 %copy-start.42 = (f32[128]{0:T(128)S(1)}, f32[128]{0:T(128)}, u32[]{:S(2)}) copy-start(f32[128]{0:T(128)} %param.33) | copy-start | bytes 1540
  298.9 9.9 %copy-start.43 = (f32[128]{0:T(128)S(1)}, f32[128]{0:T(128)}, u32[]{:S(2)}) copy-start(f32[128]{0:T(128)} %param.32) | copy-start | bytes 1540
  (21 other events, 89.8 us)
Sparse Core Ops, SparseCore 0:
  9.2 41.0 all-gather.4
  248.7 39.0 all-gather.6
  320.0 38.9 reduce-scatter.1
where the time goes:
time: 368 us; the launch traced here: 366 us
  other arithmetic  108 us (29%)
  waiting for transfers between devices  103 us (28%)
  matrix products  84.4 us (23%)
  local copies, waits for them, and re-layouts  24.7 us (7%)
  between operations  14.6 us (4%)
  blocking collectives  13.6 us (4%)
  loops' own time  10.6 us (3%)
  starting transfers between devices  6.06 us (2%)
    another operation x4, other arithmetic, block_terms(): jax.scipy.linalg.solve_triangular(identity + lower, right, lower=True, un...  78.7 us
    reduce_scatter x1, waiting for transfers between devices, local(): lax.psum_scatter((summed + jnp.dot(conv_mixed, out_conv, preferred_elemen...  39.1 us
    all_gather x1, waiting for transfers between devices, local(): piece = lax.all_gather(tokens, 'tp', axis=1, tiled=True)  39.1 us
    dot_general x16, matrix products, advance(): output = output + jnp.einsum('hcs,hse->hce', scores_block, fresh)  23.6 us
    exp x16, other arithmetic, advance(): jnp.exp(log_block)[..., None]  20.1 us
    dot_general x7, matrix products, local(): jnp.dot(piece, weight, preferred_element_type=jnp.float32)  15.6 us
    all_gather x1, waiting for transfers between devices, prefix_by_axis(): pieces = lax.all_gather(so_far, axis)  15.2 us
    all_gather x1, blocking collectives, prefix_by_axis(): pieces = lax.all_gather(so_far, axis)  13.6 us
  transfers between devices with their start and end apart: 5, of which 5 were waited for; matrix products, arithmetic and copies ran while one was open for 3% of the time, Pallas kernels for 0%

commit v1 on v0

--- a/solution.py
+++ b/solution.py
@@ -109,7 +109,9 @@
         w_beta,
         w_decay,
     )
-    piece = lax.all_gather(tokens, "tp", axis=1, tiled=True)
+    piece = jnp.concatenate(
+        lax.all_to_all(jnp.stack([tokens] * lax.axis_size("tp")), "tp", 0, 0), axis=1
+    )
     totals = tuple(
         (jnp.dot(piece, weight, preferred_element_type=jnp.float32) for weight in weights)
     )

time: 368 us -> 391 us (1.062)
  matrix products: 84.4 us -> 92.8 us
  starting transfers between devices: 6.06 us -> 12.4 us
  waiting for transfers between devices: 103 us -> 107 us
    all_to_all x0 -> x1, waiting for transfers between devices: none -> 47.4 us  [local(): lax.all_to_all(jnp.stack([tokens] * lax.axis_size('tp')), 'tp', 0, 0)]
    all_gather x1 -> x0, waiting for transfers between devices: 39.1 us -> none  [local(): piece = lax.all_gather(tokens, 'tp', axis=1, tiled=True)]
    dot_general x7, matrix products: 15.6 us -> 23.8 us  [local(): jnp.dot(piece, weight, preferred_element_type=jnp.float32)]
    all_to_all x0 -> x1, starting transfers between devices: none -> 4.72 us  [local(): lax.all_to_all(jnp.stack([tokens] * lax.axis_size('tp')), 'tp', 0, 0)]
where the time goes in v1:
time: 391 us; the launch traced here: 388 us
  other arithmetic  108 us (28%)
  waiting for transfers between devices  107 us (27%)
  matrix products  92.8 us (24%)
  local copies, waits for them, and re-layouts  27.5 us (7%)
  between operations  14.9 us (4%)
  blocking collectives  13 us (3%)
  starting transfers between devices  12.4 us (3%)
  loops' own time  11.9 us (3%)
    another operation x4, other arithmetic, block_terms(): jax.scipy.linalg.solve_triangular(identity + lower, right, lower=True, un...  78.7 us
    all_to_all x1, waiting for transfers between devices, local(): lax.all_to_all(jnp.stack([tokens] * lax.axis_size('tp')), 'tp', 0, 0)  47.4 us
    reduce_scatter x1, waiting for transfers between devices, local(): lax.psum_scatter((summed + jnp.dot(conv_mixed, out_conv, preferred_elemen...  39.1 us
    dot_general x7, matrix products, local(): jnp.dot(piece, weight, preferred_element_type=jnp.float32)  23.8 us
    dot_general x16, matrix products, advance(): output = output + jnp.einsum('hcs,hse->hce', scores_block, fresh)  23.7 us
    exp x16, other arithmetic, advance(): jnp.exp(log_block)[..., None]  21.2 us
    all_gather x1, waiting for transfers between devices, prefix_by_axis(): pieces = lax.all_gather(so_far, axis)  13.9 us
    all_gather x1, blocking collectives, prefix_by_axis(): pieces = lax.all_gather(so_far, axis)  13 us
  transfers between devices with their start and end apart: 5, of which 5 were waited for; matrix products, arithmetic and copies ran while one was open for 3% of the time, Pallas kernels for 0%

profile of v1, /device:TPU:2, one launch (start us, length us, event | category | flops | bytes accessed | tf_op | source)
XLA Modules:
  0.0 388.2 jit_solution(10961715103665539064)
XLA Ops:
  7.8 2.5 stack.2
  10.4 4.7 %all-to-all-start = ((bf16[8,1024,256]{1,2,0:T(8,128)(2,1)}), bf16[8,1024,256]{1,2,0:T(8,128)(2,1)}, u32[]{:S(2)}, u32[]{:S(2)}) async-start(bf16[8,1024,256]{1,2,0:T(8,128)(2,1)} %stack.2), calls=%async_computation | async-start | bytes 8388608 | tf_op jit(solution)/shard_map/all_to_all | solution.py:113
  17.3 47.4 %all-to-all-done = bf16[8,1024,256]{1,2,0:T(8,128)(2,1)} async-done(((bf16[8,1024,256]{1,2,0:T(8,128)(2,1)}), bf16[8,1024,256]{1,2,0:T(8,128)(2,1)}, u32[]{:S(2)}, u32[]{:S(2)}) %all-to-all-start) | async-done | bytes 4194336 | tf_op jit(solution)/shard_map/all_to_all | solution.py:113
  64.7 3.1 multiply_reduce_fusion
  67.9 2.9 fusion.198
  70.8 2.9 fusion.197
  74.1 3.5 fusion.34
  77.6 3.6 multiply_reduce_fusion.4
  82.0 78.6 %custom-call.4 = f32[16,1,64,64]{2,3,1,0:T(8,128)S(1)} custom-call(f32[16,1,64,64]{3,2,1,0:T(8,128)S(1)} %fusion.30), custom_call_target="InvertDiagBlocksLowerTriangular" | custom-call | tf_op jit(solution)/shard_map/jit(_solve_triangular)/vmap()/triangular_solve | solution.py:71
  162.3 3.8 multiply_reduce_fusion.3
  168.5 87.7 %while.12 = (s32[]{:T(128)}, f32[1,128,256]{2,1,0:T(8,128)S(1)}, f32[16,1,64,256]{3,2,1,0:T(8,128)}, f32[16,1,64]{2,1,0:T(1,128)}, f32[16,1,64,128]{3,2,1,0:T(8,...) while((s32[]{:T(128)}, f32[1,128,256]{2,1,0:T(8,128)S(1)}, ...), condition=%wide.region_5.6_spmd, body=%wide.region_4.5_spmd.sunk | while | flops 14811202 | bytes 1019293 | solution.py:173
  172.5 1.5 fusion.250
  189.0 1.5 fusion.250
  199.7 1.5 fusion.250
  210.7 1.5 fusion.250
  216.2 1.5 fusion.250
  227.1 1.5 fusion.250
  238.1 1.5 fusion.250
  254.7 1.5 fusion.250
  256.1 13.0 %all-gather = f32[4,128,256]{2,1,0:T(8,128)S(1)} all-gather(f32[1,128,256]{2,1,0:T(8,128)S(1)} %get-tuple-element.54), channel_id=2, replica_groups=mesh['sp_0'=8,'sp_1'=4,'tp'=8] {'sp_1'}, dimensions={0}, use_global_device_ids=true | all-gather | bytes 655360 | tf_op jit(solution)/shard_map/all_gather | solution.py:23
  270.5 3.6 fusion.48
  274.3 3.5 fusion.42
  277.9 4.3 %collective-permute-start = (bf16[30,128]{1,0:T(8,128)(2,1)S(1)}, bf16[30,128]{1,0:T(8,128)(2,1)S(1)}, u32[]{:S(2)}, u32[]{:S(2)}) collective-permute-start(bf16[30,128]{1,0:T(8,128)(2,1)S(1)} %slice.504), channel_id=1, source_target_pairs={{0,8},{8,16},{16,24},{24,32},{32,40},{40,48},{48,56},{56,64},{64,7... | collective-permute-start | bytes 23048 | tf_op jit(solution)/shard_map/ppermute | solution.py:36
  282.2 1.5 collective-permute-done
  283.9 2.7 fusion.188
  287.3 3.3 all-to-all-start.1
  290.9 5.3 %all-to-all-done.1 = f32[8,1,2048]{2,1,0:T(1,128)S(1)} async-done(((f32[8,1,2048]{2,1,0:T(1,128)}), f32[8,1,2048]{2,1,0:T(1,128)S(1)}, u32[]{:S(2)}, u32[]{:S(2)}) %all-to-all-start.1) | async-done | bytes 65568 | tf_op jit(solution)/shard_map/all_to_all | solution.py:41
  296.3 13.9 %all-gather.4.cloned.1.call-done = f32[8,128,256]{2,1,0:T(8,128)} async-done(((f32[1,128,256]{2,1,0:T(8,128)}), f32[8,128,256]{2,1,0:T(8,128)}) %all-gather.4.cloned.1.call-update) | async-done | bytes 1048592 | tf_op jit(solution)/shard_map/all_gather | solution.py:23
  318.2 1.8 convolution_bitcast_fusion.4
  321.4 9.9 %fusion.81 = f32[1024,2048]{1,0:T(8,128)} fusion(bf16[128,2048]{1,0:T(8,128)(2,1)S(1)} %copy-done, f32[1,1024,128]{2,1,0:T(8,128)S(1)} %get-tuple-element.177, bf16[1024,2048]{0,1:T(8,128)(2,1)} %bitcast.17, bf16[2048,128]{1,0:T(8,128)(2,1)S(1)} %copy-done.5, f32[128]{0:T(128)S(1)} %copy-done.37, f32[1024]{0:T(1024)S(1)} %add_rsqrt_fusion, ...), kind=kOutput, calls=%fused_computation.153 | convolution fusion | flops 1075183616 | bytes 14164480 | tf_op jit(solution)/shard_map/dot_general | solution.py:221
  331.3 11.0 %add_convert_fusion = bf16[1024,2048]{1,0:T(8,128)(2,1)} fusion(f32[1024,2048]{1,0:T(8,128)} %fusion.81, bf16[128,2048]{1,0:T(8,128)(2,1)S(1)} %copy-done.3, bf16[1024,2048]{0,1:T(8,128)(2,1)} %bitcast.17, bf16[2048,128]{1,0:T(8,128)(2,1)S(1)} %copy-done.4, f32[1024,128]{1,0:T(8,128)S(1)} %get-tuple-element.122, f32[128]{0:T(128)S(1)} %copy-done.35, ...), kind=kOutput, calls=%fused_computation.32 | convolution fusion | flops 1080164352 | bytes 18363392 | tf_op jit(solution)/shard_map/dot_general | solution.py:223
  342.3 39.1 %reduce-scatter.2.cloned.1.call-done = bf16[128,2048]{1,0:T(8,128)(2,1)} async-done(((bf16[1024,2048]{1,0:T(8,128)(2,1)}), bf16[128,2048]{1,0:T(8,128)(2,1)}) %reduce-scatter.2.cloned.1.call-update) | async-done | bytes 524304 | tf_op jit(solution)/shard_map/reduce_scatter | solution.py:222
  (258 shorter events, 83.5 us)
Async XLA Ops:
  6.5 314.8 %copy-start = (bf16[128,2048]{1,0:T(8,128)(2,1)S(1)}, bf16[128,2048]{1,0:T(8,128)(2,1)}, u32[]{:S(2)}) copy-start(bf16[128,2048]{1,0:T(8,128)(2,1)} %param.34) | copy-start | bytes 1572868
  10.4 54.4 %all-to-all-start = ((bf16[8,1024,256]{1,2,0:T(8,128)(2,1)}), bf16[8,1024,256]{1,2,0:T(8,128)(2,1)}, u32[]{:S(2)}, u32[]{:S(2)}) async-start(bf16[8,1024,256]{1,2,0:T(8,128)(2,1)} %stack.2), calls=%async_computation | async-start | bytes 8388608 | tf_op jit(solution)/shard_map/all_to_all | solution.py:113
  15.1 52.8 %copy-start.11 = (bf16[2048,8]{0,1:T(8,128)(2,1)S(1)}, bf16[2048,8]{0,1:T(8,128)(2,1)}, u32[]{:S(2)}) copy-start(bf16[2048,8]{0,1:T(8,128)(2,1)} %param.27) | copy-start | bytes 98308
  15.1 295.1 %all-gather.4.cloned.1.call-start = ((), (), s32[]{:S(2)}) async-start(), calls=%async_computation.4 | async-start | bytes 1179648 | tf_op jit(solution)/shard_map/all_gather | solution.py:23
  17.3 53.5 %copy-start.12 = (bf16[2048,8]{0,1:T(8,128)(2,1)S(1)}, bf16[2048,8]{0,1:T(8,128)(2,1)}, u32[]{:S(2)}) copy-start(bf16[2048,8]{0,1:T(8,128)(2,1)} %param.28) | copy-start | bytes 98308
  67.8 94.5 %copy-start.6 = (f32[1024]{0:T(1024)}, f32[1024]{0:T(1024)S(1)}, u32[]{:S(2)}) copy-start(f32[1024]{0:T(1024)S(1)} %add_rsqrt_fusion.3) | copy-start | bytes 12292
  74.1 92.1 %copy-start.10 = (f32[1,16,64]{2,1,0:T(8,128)}, f32[1,16,64]{2,1,0:T(8,128)S(1)}, u32[]{:S(2)}) copy-start(f32[1,16,64]{2,1,0:T(8,128)S(1)} %reduce_window_sum.11) | copy-start | bytes 12292
  81.3 84.9 %copy-start.9 = (f32[16,64]{1,0:T(8,128)}, f32[16,64]{1,0:T(8,128)S(1)}, u32[]{:S(2)}) copy-start(f32[16,64]{1,0:T(8,128)S(1)} %rsqrt.42) | copy-start | bytes 12292
  168.5 102.0 %copy-start.7 = (f32[1024]{0:T(1024)S(1)}, f32[1024]{0:T(1024)}, u32[]{:S(2)}) copy-start(f32[1024]{0:T(1024)} %copy-done.6) | copy-start | bytes 12292
  168.5 102.0 %copy-start.40 = (bf16[2048,128]{1,0:T(8,128)(2,1)S(1)}, bf16[2048,128]{1,0:T(8,128)(2,1)}, u32[]{:S(2)}) copy-start(bf16[2048,128]{1,0:T(8,128)(2,1)} %param.25) | copy-start | bytes 1572868
  274.1 9.6 %copy-start.16 = (f32[128]{0:T(128)S(1)}, f32[128]{0:T(128)}, u32[]{:S(2)}) copy-start(f32[128]{0:T(128)} %get-tuple-element.139) | copy-start | bytes 1540
  274.1 9.6 %copy-start.17 = (f32[128]{0:T(128)S(1)}, f32[128]{0:T(128)}, u32[]{:S(2)}) copy-start(f32[128]{0:T(128)} %get-tuple-element.140) | copy-start | bytes 1540
  274.1 9.6 %copy-start.18 = (f32[128]{0:T(128)S(1)}, f32[128]{0:T(128)}, u32[]{:S(2)}) copy-start(f32[128]{0:T(128)} %get-tuple-element.141) | copy-start | bytes 1540
  274.1 9.6 %copy-start.19 = (f32[128]{0:T(128)S(1)}, f32[128]{0:T(128)}, u32[]{:S(2)}) copy-start(f32[128]{0:T(128)} %get-tuple-element.142) | copy-start | bytes 1540
  274.2 9.6 %copy-start.20 = (f32[128]{0:T(128)S(1)}, f32[128]{0:T(128)}, u32[]{:S(2)}) copy-start(f32[128]{0:T(128)} %get-tuple-element.143) | copy-start | bytes 1540
  274.2 9.6 %copy-start.21 = (f32[128]{0:T(128)S(1)}, f32[128]{0:T(128)}, u32[]{:S(2)}) copy-start(f32[128]{0:T(128)} %get-tuple-element.144) | copy-start | bytes 1540
  274.2 9.6 %copy-start.22 = (f32[128]{0:T(128)S(1)}, f32[128]{0:T(128)}, u32[]{:S(2)}) copy-start(f32[128]{0:T(128)} %get-tuple-element.145) | copy-start | bytes 1540
  274.2 9.6 %copy-start.23 = (f32[128]{0:T(128)S(1)}, f32[128]{0:T(128)}, u32[]{:S(2)}) copy-start(f32[128]{0:T(128)} %get-tuple-element.146) | copy-start | bytes 1540
  274.2 9.6 %copy-start.24 = (f32[128]{0:T(128)S(1)}, f32[128]{0:T(128)}, u32[]{:S(2)}) copy-start(f32[128]{0:T(128)} %get-tuple-element.147) | copy-start | bytes 1540
  274.2 9.6 %copy-start.25 = (f32[128]{0:T(128)S(1)}, f32[128]{0:T(128)}, u32[]{:S(2)}) copy-start(f32[128]{0:T(128)} %get-tuple-element.148) | copy-start | bytes 1540
  274.2 9.6 %copy-start.26 = (f32[128]{0:T(128)S(1)}, f32[128]{0:T(128)}, u32[]{:S(2)}) copy-start(f32[128]{0:T(128)} %get-tuple-element.149) | copy-start | bytes 1540
  274.3 16.4 %copy-start.1 = (f32[1,128,256]{2,1,0:T(8,128)S(1)}, f32[1,128,256]{2,1,0:T(8,128)}, u32[]{:S(2)}) copy-start(f32[1,128,256]{2,1,0:T(8,128)} %fusion.53) | copy-start | bytes 393220
  277.8 42.2 %copy-start.8 = (f32[16,1,64,256]{3,2,1,0:T(8,128)S(1)}, f32[16,1,64,256]{3,2,1,0:T(8,128)}, u32[]{:S(2)}) copy-start(f32[16,1,64,256]{3,2,1,0:T(8,128)} %get-tuple-element.53) | copy-start | bytes 3145732
  277.9 43.4 %copy-start.5 = (bf16[2048,128]{1,0:T(8,128)(2,1)S(1)}, bf16[2048,128]{1,0:T(8,128)(2,1)}, u32[]{:S(2)}) copy-start(bf16[2048,128]{1,0:T(8,128)(2,1)} %param.23) | copy-start | bytes 1572868
  277.9 43.4 %copy-start.37 = (f32[128]{0:T(128)S(1)}, f32[128]{0:T(128)}, u32[]{:S(2)}) copy-start(f32[128]{0:T(128)} %param.30) | copy-start | bytes 1540
  277.9 5.9 %collective-permute-start = (bf16[30,128]{1,0:T(8,128)(2,1)S(1)}, bf16[30,128]{1,0:T(8,128)(2,1)S(1)}, u32[]{:S(2)}, u32[]{:S(2)}) collective-permute-start(bf16[30,128]{1,0:T(8,128)(2,1)S(1)} %slice.504), channel_id=1, source_target_pairs={{0,8},{8,16},{16,24},{24,32},{32,40},{40,48},{48,56},{56,64},{64,7... | collective-permute-start | bytes 23048 | tf_op jit(solution)/shard_map/ppermute | solution.py:36
  287.3 8.9 %all-to-all-start.1 = ((f32[8,1,2048]{2,1,0:T(1,128)}), f32[8,1,2048]{2,1,0:T(1,128)S(1)}, u32[]{:S(2)}, u32[]{:S(2)}) async-start(f32[8,1,2048]{2,1,0:T(1,128)} %broadcast_in_dim.36), calls=%async_computation.1 | async-start | bytes 131072 | tf_op jit(solution)/shard_map/all_to_all | solution.py:41
  290.7 90.7 %reduce-scatter.2.cloned.1.call-start = ((), (), s32[]{:S(2)}) async-start(), calls=%async_computation.3 | async-start | bytes 4718592 | tf_op jit(solution)/shard_map/reduce_scatter | solution.py:222
  321.3 10.0 %copy-start.3 = (bf16[128,2048]{1,0:T(8,128)(2,1)S(1)}, bf16[128,2048]{1,0:T(8,128)(2,1)}, u32[]{:S(2)}) copy-start(bf16[128,2048]{1,0:T(8,128)(2,1)} %param.35) | copy-start | bytes 1572868
  321.3 10.0 %copy-start.4 = (bf16[2048,128]{1,0:T(8,128)(2,1)S(1)}, bf16[2048,128]{1,0:T(8,128)(2,1)}, u32[]{:S(2)}) copy-start(bf16[2048,128]{1,0:T(8,128)(2,1)} %param.26) | copy-start | bytes 1572868
  321.3 10.0 %copy-start.35 = (f32[128]{0:T(128)S(1)}, f32[128]{0:T(128)}, u32[]{:S(2)}) copy-start(f32[128]{0:T(128)} %param.33) | copy-start | bytes 1540
  321.4 10.0 %copy-start.36 = (f32[128]{0:T(128)S(1)}, f32[128]{0:T(128)}, u32[]{:S(2)}) copy-start(f32[128]{0:T(128)} %param.32) | copy-start | bytes 1540
  (15 other events, 113.9 us)
Sparse Core Ops, SparseCore 0:
  270.6 39.5 all-gather.3
  342.4 38.9 reduce-scatter.1
